TPU v7x, 32 devices: a whole 2x2x4 slice. The times are simulated.
32 devices in a mesh: tp: 8 (over z, x), dp: 4 (over y, core).
Axes of the slice: x: 2, y: 2, z: 4, core: 2. Of those that a mesh axis runs over, the one named last changes fastest.
Arguments:
- stream: bfloat16 [128, 4096], P(None, 'dp'), may hold values from -12 to 12
- history: int32 [128], P('dp'), may hold values from 1 to 4096, 131072 in all
- input_norm_gain: float32 [2, 4096], P(None, 'dp'), may hold values from 0.1 to 1.9
- query_weight: bfloat16 [2, 4096, 4096], P(None, 'dp', 'tp'), may hold values from -0.09375 to 0.09375
- key_weight: bfloat16 [2, 4096, 4096], P(None, 'dp', 'tp'), may hold values from -0.09375 to 0.09375
- value_weight: bfloat16 [2, 4096, 4096], P(None, 'dp', 'tp'), may hold values from -0.09375 to 0.09375
- gate_weight: bfloat16 [2, 4096, 4096], P(None, 'dp', 'tp'), may hold values from -0.09375 to 0.09375
- adapter_down_weight: bfloat16 [2, 4096, 128], P(None, 'dp'), may hold values from -0.09375 to 0.09375
- decay_up_weight: float32 [2, 64, 4096], P(None, None, 'tp'), may hold values from -3 to 3
- rate_up_weight: float32 [2, 64, 4096], P(None, None, 'tp'), may hold values from -3 to 3
- decay_offset: float32 [2, 4096], P(None, 'tp'), may hold values from -3 to 1
- head_norm_gain: float32 [2, 4096], P(None, 'tp'), may hold values from 0.1 to 1.9
- output_weight: bfloat16 [2, 4096, 4096], P(None, 'tp', 'dp'), may hold values from -0.09375 to 0.09375
- recurrent_state: float32 [2, 128, 64, 4096], P(None, 'dp', 'tp'), may hold values from -5 to 5
Outputs:
- stream_out: bfloat16 [128, 4096], P(None, 'dp')
- state_out: float32 [2, 128, 64, 4096], P(None, 'dp', 'tp')
All inputs are finite; a program needn't handle non-finite values. No bound on the sum of `history` on one device may be relied on, other than what follows from the above.
Results may differ from a plain program's by a relative error of at most 0.024.
Values may be sent and summed in bfloat16 or wider, within the bound.
No kernel may reach another device: no remote copies, remote signals or barrier semaphores. Data moves between devices by JAX's collectives and lax.ppermute only.
A program may use at most 128 MiB of HBM per device.

v0:
```python
import jax
import jax.numpy as jnp
from jax import lax
from jax.sharding import PartitionSpec as P

MODEL_WIDTH = 4096
HEAD = 64
ADAPTER_RANK = 64
SPAN = 64
BLOCK_COUNT = 2


NORM_EPS = 0.25
GROUP_EPS = 0.25


def truncated_product(rescaled_rows, weight):
    product = jnp.dot(rescaled_rows, weight, preferred_element_type=jnp.float32).astype(
        jnp.bfloat16
    )
    return lax.optimization_barrier(product).astype(jnp.float32)


def recur_heads(
    query,
    key_proj,
    value_proj,
    gate_pre,
    adapter_hidden,
    pos_factor,
    decay_up_weight,
    rate_up_weight,
    decay_offset,
    head_norm_gain,
    recurrent_state,
):
    seq_local, width = query.shape
    head_count = width // HEAD
    decay_logits = decay_offset[None, :] + jnp.dot(
        jnp.tanh(adapter_hidden[:, :ADAPTER_RANK]), decay_up_weight, precision=lax.Precision.HIGHEST
    )
    rate_log = -jax.nn.softplus(-decay_logits) - 0.5
    decay = jnp.exp(-jnp.exp(rate_log) * pos_factor)
    learning_rate = jax.nn.sigmoid(
        jnp.dot(adapter_hidden[:, ADAPTER_RANK:], rate_up_weight, precision=lax.Precision.HIGHEST)
    )

    def heads_of(values):
        return values.reshape(seq_local, head_count, HEAD)

    keys = heads_of(key_proj)
    key_unit = keys * lax.rsqrt(jnp.sum(keys * keys, axis=-1, keepdims=True) + 1.0)
    key_rate = key_unit * heads_of(learning_rate)
    matrix = recurrent_state.reshape(seq_local, head_count, HEAD, HEAD)
    state_key = jnp.einsum("bhvk,bhk->bhv", matrix, key_unit)
    refreshed_state = (
        matrix * heads_of(decay)[:, :, None, :]
        - state_key[..., None] * key_rate[:, :, None, :]
        + heads_of(value_proj)[..., None] * keys[:, :, None, :]
    )
    readout = jnp.einsum("bhvk,bhk->bhv", refreshed_state, heads_of(query))
    mean_y = jnp.mean(readout, axis=-1, keepdims=True)
    spread = jnp.mean(jnp.square(readout - mean_y), axis=-1, keepdims=True)
    normed = ((readout - mean_y) * lax.rsqrt(spread + GROUP_EPS)).reshape(
        seq_local, width
    ) * head_norm_gain[None, :]
    mixed = (normed * jax.nn.sigmoid(gate_pre)).astype(jnp.bfloat16)
    return (mixed, refreshed_state.reshape(seq_local, head_count, HEAD * HEAD))


def body(
    stream,
    history,
    input_norm_gain,
    query_weight,
    key_weight,
    value_weight,
    gate_weight,
    adapter_down_weight,
    decay_up_weight,
    rate_up_weight,
    decay_offset,
    head_norm_gain,
    output_weight,
    recurrent_state,
):
    seq_local = history.shape[0]
    pos_factor = (0.5 + (history // SPAN % 3).astype(jnp.float32))[:, None]
    new_states = []
    for layer_lookup in range(BLOCK_COUNT):
        widened = stream.astype(jnp.float32)
        squares = jnp.sum(widened * widened, axis=1)
        rescaled_rows = (widened * input_norm_gain[layer_lookup][None, :]).astype(jnp.bfloat16)
        query_part = truncated_product(rescaled_rows, query_weight[layer_lookup])
        key_part = truncated_product(rescaled_rows, key_weight[layer_lookup])
        value_part = truncated_product(rescaled_rows, value_weight[layer_lookup])
        gate_part = truncated_product(rescaled_rows, gate_weight[layer_lookup])
        adapter_section = truncated_product(rescaled_rows, adapter_down_weight[layer_lookup])
        totals = lax.psum(squares, "dp")
        summed = (
            lax.psum_scatter(
                query_part.astype(jnp.bfloat16), "dp", scatter_dimension=0, tiled=True
            ).astype(jnp.float32),
            lax.psum_scatter(
                key_part.astype(jnp.bfloat16), "dp", scatter_dimension=0, tiled=True
            ).astype(jnp.float32),
            lax.psum_scatter(
                value_part.astype(jnp.bfloat16), "dp", scatter_dimension=0, tiled=True
            ).astype(jnp.float32),
            lax.psum_scatter(
                gate_part.astype(jnp.bfloat16), "dp", scatter_dimension=0, tiled=True
            ).astype(jnp.float32),
            lax.psum_scatter(
                adapter_section.astype(jnp.bfloat16), "dp", scatter_dimension=0, tiled=True
            ).astype(jnp.float32),
        )
        own_sq = lax.dynamic_slice_in_dim(totals, lax.axis_index("dp") * seq_local, seq_local, 0)
        inverse_root_mean = lax.rsqrt(own_sq / MODEL_WIDTH + NORM_EPS)[:, None]
        query, key_proj, value_proj, gate_pre, adapter_hidden = [
            part_sum * inverse_root_mean for part_sum in summed
        ]
        mixed, refreshed_state = recur_heads(
            query,
            key_proj,
            value_proj,
            gate_pre,
            adapter_hidden,
            pos_factor,
            decay_up_weight[layer_lookup],
            rate_up_weight[layer_lookup],
            decay_offset[layer_lookup],
            head_norm_gain[layer_lookup],
            recurrent_state[layer_lookup],
        )
        new_states.append(refreshed_state)
        out_weight = output_weight[layer_lookup]
        terms = jnp.dot(
            lax.all_gather(mixed, "dp", axis=0, tiled=True),
            out_weight,
            preferred_element_type=jnp.float32,
        )
        out_total = lax.psum(terms.astype(jnp.bfloat16), "tp").astype(jnp.float32)
        stream = (widened + out_total).astype(jnp.bfloat16)
    return (stream, jnp.stack(new_states))


def solution(mesh):
    placed = (
        P(None, "dp"),
        P("dp"),
        P(None, "dp"),
        P(None, "dp", "tp"),
        P(None, "dp", "tp"),
        P(None, "dp", "tp"),
        P(None, "dp", "tp"),
        P(None, "dp", None),
        P(None, None, "tp"),
        P(None, None, "tp"),
        P(None, "tp"),
        P(None, "tp"),
        P(None, "tp", "dp"),
        P(None, "dp", "tp", None),
    )
    return jax.shard_map(
        body,
        mesh=mesh,
        in_specs=placed,
        out_specs=(P(None, "dp"), P(None, "dp", "tp", None)),
        check_vma=False,
    )
```

profile of v0, /device:TPU:0, one launch (start us, length us, event | category | flops | bytes accessed | tf_op | source)
XLA Modules:
  0.0 398.0 jit_solution(10873418411421237493)
XLA Ops:
  7.3 0.8 fusion.90
  8.0 1.9 convolution_convert_fusion.11
  10.0 2.3 convolution_convert_fusion.9
  12.3 2.3 convolution_convert_fusion.8
  14.7 2.3 convolution_convert_fusion.7
  17.0 2.3 convolution_convert_fusion.6
  19.4 0.1 fusion.39
  19.6 8.4 %psum.28 = f32[128]{0:T(128)S(1)} all-reduce(f32[128]{0:T(128)S(1)} %fusion.39), channel_id=1, replica_groups=mesh['tp'=8,'dp'=4] {'dp'}, use_global_device_ids=true, to_apply=%region_2.3 | all-reduce | flops 128 | bytes 1024 | tf_op jit(solution)/shard_map/psum | solution.py:99
  28.0 7.7 %fusion.89 = (f32[1,32,8,4096]{3,2,1,0:T(8,128)}, f32[1,32,8,4096]{3,2,1,0:T(8,128)}) fusion(f32[2,32,8,4096]{3,2,1,0:T(8,128)} %param.27), kind=kLoop, calls=%fused_computation.138 | loop fusion | bytes 16777216 | tf_op jit(solution)/shard_map/slice | solution.py:133
  35.7 7.9 %reshape_squeeze.6 = f32[32,8,64,64]{3,2,1,0:T(8,128)} reshape(f32[1,32,8,4096]{3,2,1,0:T(8,128)} %get-tuple-element.11) | data formatting | bytes 8388608 | tf_op jit(solution)/shard_map/reshape;squeeze | solution.py:54
  43.7 0.8 convert_multiply_fusion.11
  44.4 0.3 fusion.16
  44.7 0.3 fusion.71
  45.2 9.7 %reduce-scatter.13.cloned.1.call-done = bf16[32,512]{1,0:T(8,128)(2,1)} async-done(((bf16[128,512]{1,0:T(8,128)(2,1)}), bf16[32,512]{1,0:T(8,128)(2,1)}) %reduce-scatter.13.cloned.1.call-update) | async-done | bytes 32784 | tf_op jit(solution)/shard_map/reduce_scatter | solution.py:104
  54.9 22.1 %reduce-scatter.15.cloned.1.call-done = bf16[32,512]{1,0:T(8,128)(2,1)} async-done(((bf16[128,512]{1,0:T(8,128)(2,1)}), bf16[32,512]{1,0:T(8,128)(2,1)}) %reduce-scatter.15.cloned.1.call-update) | async-done | bytes 32784 | tf_op jit(solution)/shard_map/reduce_scatter | solution.py:107
  77.0 22.0 %reduce-scatter.17.cloned.1.call-done = bf16[32,512]{1,0:T(8,128)(2,1)} async-done(((bf16[128,512]{1,0:T(8,128)(2,1)}), bf16[32,512]{1,0:T(8,128)(2,1)}) %reduce-scatter.17.cloned.1.call-update) | async-done | bytes 32784 | tf_op jit(solution)/shard_map/reduce_scatter | solution.py:101
  98.9 0.9 convert_multiply_fusion.8
  100.3 5.8 %fusion.93 = f32[32,8,1,64]{3,2,1,0:T(1,128)S(1)} fusion(f32[32,8,64,1]{2,3,1,0:T(1,128)S(1)} %bitcast.110, f32[32,8,64,64]{3,2,1,0:T(8,128)} %reshape_squeeze.6), kind=kOutput, calls=%fused_computation.142 | convolution fusion | flops 2097152 | bytes 4325376 | tf_op jit(solution)/shard_map/bhvk,bhk->bhv/dot_general | solution.py:55
  106.1 5.8 %fusion.4 = f32[32,8,1,64]{3,2,1,0:T(1,128)S(1)} fusion(f32[32,8,64,1]{2,3,1,0:T(1,128)S(1)} %bitcast.113, f32[32,8,64,64]{3,2,1,0:T(8,128)S(1)} %copy-done, f32[32,8,64]{2,1,0:T(8,128)S(1)} %mul.333, f32[32,8,64]{2,1,0:T(8,128)S(1)} %get-tuple-element.6, f32[32,8,64]{2,1,0:T(8,128)S(1)} %bitcast.106, f32[32,8,64]{2,1,0:T(8,128)S(1)} %reshape.189, ...), kind=kOutput, calls=%fused_computation.5 | convolution fusion | flops 7340032 | bytes 4653056 | tf_op jit(solution)/shard_map/bhvk,bhk->bhv/dot_general | solution.py:61
  112.1 0.2 multiply_reduce_fusion.2
  112.3 0.1 subtract_multiply_fusion.1
  112.5 9.0 %reduce-scatter.19.cloned.1.call-done = bf16[32,512]{1,0:T(8,128)(2,1)} async-done(((bf16[128,512]{1,0:T(8,128)(2,1)}), bf16[32,512]{1,0:T(8,128)(2,1)}) %reduce-scatter.19.cloned.1.call-update) | async-done | bytes 32784 | tf_op jit(solution)/shard_map/reduce_scatter | solution.py:110
  121.5 0.9 multiply_convert_fusion.1
  122.3 5.4 %all_gather.6 = bf16[128,512]{1,0:T(8,128)(2,1)S(1)} all-gather(bf16[32,512]{1,0:T(8,128)(2,1)S(1)} %multiply_convert_fusion.1), channel_id=1, replica_groups=mesh['tp'=8,'dp'=4] {'dp'}, dimensions={0}, use_global_device_ids=true | all-gather | bytes 163840 | tf_op jit(solution)/shard_map/all_gather | solution.py:138
  127.8 1.0 convolution_convert_fusion.1
  128.8 7.9 %reshape_squeeze.7 = f32[32,8,64,64]{3,2,1,0:T(8,128)} reshape(f32[1,32,8,4096]{3,2,1,0:T(8,128)} %get-tuple-element.10) | data formatting | bytes 8388608 | tf_op jit(solution)/shard_map/reshape;squeeze | solution.py:54
  136.7 3.8 mul.334
  140.5 8.1 %mul.390 = f32[1,32,8,4096]{3,2,1,0:T(8,128)} reshape(f32[32,8,64,64]{3,2,1,0:T(8,128)} %mul.334) | data formatting | bytes 8388608 | tf_op jit(solution)/shard_map/mul | solution.py:57
  148.5 51.4 %all-reduce.3.cloned.1.call-done = bf16[128,1024]{1,0:T(8,128)(2,1)} async-done(((bf16[128,1024]{1,0:T(8,128)(2,1)}), bf16[128,1024]{1,0:T(8,128)(2,1)}) %all-reduce.3.cloned.1.call-update) | async-done | bytes 262160 | tf_op jit(solution)/shard_map/psum | solution.py:142
  200.0 1.1 fusion.42
  201.1 1.8 convolution_convert_fusion.10
  203.0 1.0 convolution_convert_fusion.4
  204.0 4.6 %broadcast_multiply_fusion.2 = f32[32,8,64,64]{3,2,1,0:T(8,128)} fusion(f32[32,8,64]{2,1,0:T(8,128)S(1)} %reshape.189, f32[32,8,64]{2,1,0:T(8,128)S(1)} %mul.346), kind=kLoop, calls=%fused_computation.14 | loop fusion | flops 1048576 | bytes 4325376 | tf_op jit(solution)/shard_map/mul | solution.py:59
  208.6 1.0 convolution_convert_fusion.3
  209.5 0.2 reduce-scatter.23.cloned.1.call-start
  209.8 4.6 %broadcast_multiply_fusion.3 = f32[32,8,64,64]{3,2,1,0:T(8,128)} fusion(f32[32,8,64]{2,1,0:T(8,128)S(1)} %get-tuple-element.6, f32[32,8,64]{2,1,0:T(8,128)S(1)} %bitcast.107), kind=kLoop, calls=%fused_computation.15 | loop fusion | flops 1048576 | bytes 4325376 | tf_op jit(solution)/shard_map/mul | solution.py:58
  214.4 7.9 %mul.393 = f32[1,32,8,4096]{3,2,1,0:T(8,128)} reshape(f32[32,8,64,64]{3,2,1,0:T(8,128)} %broadcast_multiply_fusion.2) | data formatting | bytes 8388608 | tf_op jit(solution)/shard_map/mul | solution.py:59
  222.3 8.0 %mul.392 = f32[1,32,8,4096]{3,2,1,0:T(8,128)} reshape(f32[32,8,64,64]{3,2,1,0:T(8,128)} %broadcast_multiply_fusion.3) | data formatting | bytes 8388608 | tf_op jit(solution)/shard_map/mul | solution.py:58
  230.3 1.0 convolution_convert_fusion.5
  231.4 2.2 convolution_convert_fusion.2
  233.6 5.6 %psum.30 = f32[128]{0:T(128)S(1)} all-reduce(f32[128]{0:T(128)S(1)} %get-tuple-element.4), channel_id=1, replica_groups=mesh['tp'=8,'dp'=4] {'dp'}, use_global_device_ids=true, to_apply=%region_13.14 | all-reduce | flops 128 | bytes 1024 | tf_op jit(solution)/shard_map/psum | solution.py:99
  239.4 0.8 convert_multiply_fusion.10
  240.2 0.3 fusion.12
  240.4 0.3 fusion.77
  240.9 3.8 mul.366
  244.7 7.9 %mul.394 = f32[1,32,8,4096]{3,2,1,0:T(8,128)} reshape(f32[32,8,64,64]{3,2,1,0:T(8,128)} %mul.366) | data formatting | bytes 8388608 | tf_op jit(solution)/shard_map/mul | solution.py:57
  252.5 13.5 %reduce-scatter.27.cloned.1.call-done = bf16[32,512]{1,0:T(8,128)(2,1)} async-done(((bf16[128,512]{1,0:T(8,128)(2,1)}), bf16[32,512]{1,0:T(8,128)(2,1)}) %reduce-scatter.27.cloned.1.call-update) | async-done | bytes 32784 | tf_op jit(solution)/shard_map/reduce_scatter | solution.py:101
  266.0 22.0 %reduce-scatter.23.cloned.1.call-done = bf16[32,512]{1,0:T(8,128)(2,1)} async-done(((bf16[128,512]{1,0:T(8,128)(2,1)}), bf16[32,512]{1,0:T(8,128)(2,1)}) %reduce-scatter.23.cloned.1.call-update) | async-done | bytes 32784 | tf_op jit(solution)/shard_map/reduce_scatter | solution.py:104
  288.0 0.9 convert_multiply_fusion.5
  289.3 4.7 %broadcast_multiply_fusion = f32[32,8,64,64]{3,2,1,0:T(8,128)} fusion(f32[32,8,64]{2,1,0:T(8,128)S(1)} %reshape.193, f32[32,8,64]{2,1,0:T(8,128)S(1)} %mul.378), kind=kLoop, calls=%fused_computation.11 | loop fusion | flops 1048576 | bytes 4325376 | tf_op jit(solution)/shard_map/mul | solution.py:59
  294.1 5.8 %fusion.94 = f32[32,8,1,64]{3,2,1,0:T(1,128)S(1)} fusion(f32[32,8,64,1]{2,3,1,0:T(1,128)S(1)} %bitcast.111, f32[32,8,64,64]{3,2,1,0:T(8,128)} %reshape_squeeze.7), kind=kOutput, calls=%fused_computation.143 | convolution fusion | flops 2097152 | bytes 4325376 | tf_op jit(solution)/shard_map/bhvk,bhk->bhv/dot_general | solution.py:55
  299.9 5.8 %fusion = f32[32,8,1,64]{3,2,1,0:T(1,128)S(1)} fusion(f32[32,8,64,1]{2,3,1,0:T(1,128)S(1)} %bitcast.112, f32[32,8,64,64]{3,2,1,0:T(8,128)S(1)} %bitcast.99, f32[32,8,64]{2,1,0:T(8,128)S(1)} %mul.365, f32[32,8,64]{2,1,0:T(8,128)S(1)} %get-tuple-element.2, f32[32,8,64]{2,1,0:T(8,128)S(1)} %bitcast.108, f32[32,8,64]{2,1,0:T(8,128)S(1)} %reshape.193, ...), kind=kOutput, calls=%fused_computation.1 | convolution fusion | flops 7340032 | bytes 4653056 | tf_op jit(solution)/shard_map/bhvk,bhk->bhv/dot_general | solution.py:61
  305.9 0.2 multiply_reduce_fusion
  306.1 0.1 subtract_multiply_fusion
  306.3 4.6 %broadcast_multiply_fusion.1 = f32[32,8,64,64]{3,2,1,0:T(8,128)} fusion(f32[32,8,64]{2,1,0:T(8,128)S(1)} %get-tuple-element.2, f32[32,8,64]{2,1,0:T(8,128)S(1)} %bitcast.109), kind=kLoop, calls=%fused_computation.12 | loop fusion | flops 1048576 | bytes 4325376 | tf_op jit(solution)/shard_map/mul | solution.py:58
  310.9 0.9 multiply_convert_fusion
  311.7 5.4 %all_gather.7 = bf16[128,512]{1,0:T(8,128)(2,1)S(1)} all-gather(bf16[32,512]{1,0:T(8,128)(2,1)S(1)} %multiply_convert_fusion), channel_id=1, replica_groups=mesh['tp'=8,'dp'=4] {'dp'}, dimensions={0}, use_global_device_ids=true | all-gather | bytes 163840 | tf_op jit(solution)/shard_map/all_gather | solution.py:138
  317.2 1.0 convolution_convert_fusion
  318.2 7.9 %mul.397 = f32[1,32,8,4096]{3,2,1,0:T(8,128)} reshape(f32[32,8,64,64]{3,2,1,0:T(8,128)} %broadcast_multiply_fusion) | data formatting | bytes 8388608 | tf_op jit(solution)/shard_map/mul | solution.py:59
  326.1 7.9 %mul.396 = f32[1,32,8,4096]{3,2,1,0:T(8,128)} reshape(f32[32,8,64,64]{3,2,1,0:T(8,128)} %broadcast_multiply_fusion.1) | data formatting | bytes 8388608 | tf_op jit(solution)/shard_map/mul | solution.py:58
  334.1 12.3 %subtract_add_fusion.1 = (f32[1,32,8,4096]{3,2,1,0:T(8,128)S(1)}, f32[1,32,8,4096]{3,2,1,0:T(8,128)S(1)}) fusion(f32[1,32,8,4096]{3,2,1,0:T(8,128)} %mul.393, f32[1,32,8,4096]{3,2,1,0:T(8,128)} %mul.392, f32[1,32,8,4096]{3,2,1,0:T(8,128)} %mul.390, f32[2,32,8,4096]{3,2,1,0:T(8,128)} %param.27, f32[1,32,8,4096]{3,2,1,0:T(8,128)} %mul.397, ...), kind=kLoop, calls=%fused_computation.10 | loop fusion | flops 6291456 | bytes 41943040 | tf_op jit(solution)/shard_map/add | solution.py:57
  346.4 3.9 pad_maximum_fusion
  350.3 39.1 %all-reduce.5.cloned.1.call-done = bf16[128,1024]{1,0:T(8,128)(2,1)} async-done(((bf16[128,1024]{1,0:T(8,128)(2,1)}), bf16[128,1024]{1,0:T(8,128)(2,1)}) %all-reduce.5.cloned.1.call-update) | async-done | bytes 262160 | tf_op jit(solution)/shard_map/psum | solution.py:142
  389.4 1.7 fusion.43
  (89 shorter events, 2.7 us)
Async XLA Ops:
  7.2 12.2 %copy-start.1 = (bf16[128,1024]{1,0:T(8,128)(2,1)S(1)}, bf16[128,1024]{1,0:T(8,128)(2,1)}, u32[]{:S(2)}) copy-start(bf16[128,1024]{1,0:T(8,128)(2,1)} %param.14) | copy-start | bytes 786436
  7.2 12.4 %copy-start.13 = (s32[32]{0:T(128)S(1)}, s32[32]{0:T(128)}, u32[]{:S(2)}) copy-start(s32[32]{0:T(128)} %param.15) | copy-start | bytes 388
  7.2 20.8 %copy-start.2 = (f32[2,512]{1,0:T(2,128)S(1)}, f32[2,512]{1,0:T(2,128)}, u32[]{:S(2)}) copy-start(f32[2,512]{1,0:T(2,128)} %param.24) | copy-start | bytes 12292
  7.2 20.8 %copy-start.3 = (f32[2,512]{1,0:T(2,128)S(1)}, f32[2,512]{1,0:T(2,128)}, u32[]{:S(2)}) copy-start(f32[2,512]{1,0:T(2,128)} %param.25) | copy-start | bytes 12292
  7.2 36.5 %reduce-scatter.11.cloned.1.call-start = ((), (), s32[]{:S(2)}) async-start(), calls=%async_computation.10 | async-start | bytes 40960 | tf_op jit(solution)/shard_map/reduce_scatter | solution.py:113
  9.9 45.0 %reduce-scatter.13.cloned.1.call-start = ((), (), s32[]{:S(2)}) async-start(), calls=%async_computation.11 | async-start | bytes 163840 | tf_op jit(solution)/shard_map/reduce_scatter | solution.py:104
  12.3 64.7 %reduce-scatter.15.cloned.1.call-start = ((), (), s32[]{:S(2)}) async-start(), calls=%async_computation.12 | async-start | bytes 163840 | tf_op jit(solution)/shard_map/reduce_scatter | solution.py:107
  14.6 84.3 %reduce-scatter.17.cloned.1.call-start = ((), (), s32[]{:S(2)}) async-start(), calls=%async_computation.13 | async-start | bytes 163840 | tf_op jit(solution)/shard_map/reduce_scatter | solution.py:101
  17.0 104.5 %reduce-scatter.19.cloned.1.call-start = ((), (), s32[]{:S(2)}) async-start(), calls=%async_computation.14 | async-start | bytes 163840 | tf_op jit(solution)/shard_map/reduce_scatter | solution.py:110
  19.3 180.6 %all-reduce.3.cloned.1.call-start = ((), (), s32[]{:S(2)}) async-start(), calls=%async_computation.15 | async-start | bytes 524288 | tf_op jit(solution)/shard_map/psum | solution.py:142
  35.7 8.8 %copy-start.9 = (f32[2,64,512]{2,1,0:T(8,128)S(1)}, f32[2,64,512]{2,1,0:T(8,128)}, u32[]{:S(2)}) copy-start(f32[2,64,512]{2,1,0:T(8,128)} %param.23) | copy-start | bytes 786436
  35.7 9.0 %copy-start.11 = (f32[2,64,512]{2,1,0:T(8,128)S(1)}, f32[2,64,512]{2,1,0:T(8,128)}, u32[]{:S(2)}) copy-start(f32[2,64,512]{2,1,0:T(8,128)} %param.22) | copy-start | bytes 786436
  100.2 5.9 %copy-start = (f32[32,8,64,64]{3,2,1,0:T(8,128)S(1)}, f32[32,8,64,64]{3,2,1,0:T(8,128)}, u32[]{:S(2)}) copy-start(f32[32,8,64,64]{3,2,1,0:T(8,128)} %reshape_squeeze.6) | copy-start | bytes 12582916
  106.1 21.6 %copy-start.7 = (bf16[2,512,1024]{2,1,0:T(8,128)(2,1)S(1)}, bf16[2,512,1024]{2,1,0:T(8,128)(2,1)}, u32[]{:S(2)}) copy-start(bf16[2,512,1024]{2,1,0:T(8,128)(2,1)} %param.26) | copy-start | bytes 6291460
  128.8 110.6 %reduce-scatter.21.cloned.1.call-start = ((), (), s32[]{:S(2)}) async-start(), calls=%async_computation.16 | async-start | bytes 40960 | tf_op jit(solution)/shard_map/reduce_scatter | solution.py:113
  140.5 62.5 %copy-start.4 = (bf16[2,1024,512]{2,1,0:T(8,128)(2,1)S(1)}, bf16[2,1024,512]{2,1,0:T(8,128)(2,1)}, u32[]{:S(2)}) copy-start(bf16[2,1024,512]{2,1,0:T(8,128)(2,1)} %param.19) | copy-start | bytes 6291460
  202.9 49.6 %reduce-scatter.25.cloned.1.call-start = ((), (), s32[]{:S(2)}) async-start(), calls=%async_computation.18 | async-start | bytes 163840 | tf_op jit(solution)/shard_map/reduce_scatter | solution.py:107
  203.9 4.6 %copy-start.5 = (bf16[2,1024,512]{2,1,0:T(8,128)(2,1)S(1)}, bf16[2,1024,512]{2,1,0:T(8,128)(2,1)}, u32[]{:S(2)}) copy-start(bf16[2,1024,512]{2,1,0:T(8,128)(2,1)} %param.17) | copy-start | bytes 6291460
  203.9 62.1 %reduce-scatter.27.cloned.1.call-start = ((), (), s32[]{:S(2)}) async-start(), calls=%async_computation.19 | async-start | bytes 163840 | tf_op jit(solution)/shard_map/reduce_scatter | solution.py:101
  209.5 78.4 %reduce-scatter.23.cloned.1.call-start = ((), (), s32[]{:S(2)}) async-start(), calls=%async_computation.17 | async-start | bytes 163840 | tf_op jit(solution)/shard_map/reduce_scatter | solution.py:104
  222.3 8.1 %copy-start.6 = (bf16[2,1024,512]{2,1,0:T(8,128)(2,1)S(1)}, bf16[2,1024,512]{2,1,0:T(8,128)(2,1)}, u32[]{:S(2)}) copy-start(bf16[2,1024,512]{2,1,0:T(8,128)(2,1)} %param.18) | copy-start | bytes 6291460
  222.3 17.9 %copy-start.10 = (f32[2,64,512]{2,1,0:T(8,128)S(1)}, f32[2,64,512]{2,1,0:T(8,128)}, u32[]{:S(2)}) copy-start(f32[2,64,512]{2,1,0:T(8,128)} %param.23) | copy-start | bytes 786436
  222.3 18.2 %copy-start.12 = (f32[2,64,512]{2,1,0:T(8,128)S(1)}, f32[2,64,512]{2,1,0:T(8,128)}, u32[]{:S(2)}) copy-start(f32[2,64,512]{2,1,0:T(8,128)} %param.22) | copy-start | bytes 786436
  231.3 79.6 %reduce-scatter.29.cloned.1.call-start = ((), (), s32[]{:S(2)}) async-start(), calls=%async_computation.20 | async-start | bytes 163840 | tf_op jit(solution)/shard_map/reduce_scatter | solution.py:110
  239.3 150.1 %all-reduce.5.cloned.1.call-start = ((), (), s32[]{:S(2)}) async-start(), calls=%async_computation.21 | async-start | bytes 524288 | tf_op jit(solution)/shard_map/psum | solution.py:142
  289.2 10.6 %slice-start = ((s8[8388608]{0:T(1024)(128)(4,1)}), s8[4194304]{0:T(1024)(128)(4,1)S(1)}, s32[]{:S(2)}) async-start(s8[8388608]{0:T(1024)(128)(4,1)} %bitcast.98), calls=%async_computation.22 | async-start | bytes 8388608
  294.0 5.9 %slice-start.1 = ((s8[8388608]{0:T(1024)(128)(4,1)}), s8[4194304]{0:T(1024)(128)(4,1)S(1)}, s32[]{:S(2)}) async-start(s8[8388608]{0:T(1024)(128)(4,1)} %bitcast.98), calls=%async_computation.23 | async-start | bytes 8388608
  299.9 17.3 %copy-start.8 = (bf16[2,512,1024]{2,1,0:T(8,128)(2,1)S(1)}, bf16[2,512,1024]{2,1,0:T(8,128)(2,1)}, u32[]{:S(2)}) copy-start(bf16[2,512,1024]{2,1,0:T(8,128)(2,1)} %param.26) | copy-start | bytes 6291460
Sparse Core Ops, SparseCore 0:
  10.4 22.3 reduce-scatter.10
  35.2 19.6 reduce-scatter.12
  57.3 19.6 reduce-scatter.14
  79.3 19.6 reduce-scatter.16
  101.8 19.6 reduce-scatter.18
  128.9 70.9 all-reduce.2
  203.0 18.7 reduce-scatter.20
  224.3 19.6 reduce-scatter.24
  246.3 19.6 reduce-scatter.26
  268.3 19.6 reduce-scatter.22
  291.0 19.6 reduce-scatter.28
  318.3 71.0 all-reduce.4
where the time goes:
time: 400 us; the launch traced here: 398 us
  waiting for transfers between devices  189 us (47%)
  local copies, waits for them, and re-layouts  80.6 us (20%)
  matrix products  44.2 us (11%)
  other arithmetic  44.1 us (11%)
  blocking collectives  24.9 us (6%)
  between operations  14.5 us (4%)
    psum x2, waiting for transfers between devices, body(): out_total = lax.psum(terms.astype(jnp.bfloat16), 'tp').astype(jnp.float32)  90.5 us
    reduce_scatter x2, waiting for transfers between devices, body(): lax.psum_scatter(query_part.astype(jnp.bfloat16), 'dp', scatter_dimension...  35.4 us
    reduce_scatter x2, waiting for transfers between devices, body(): lax.psum_scatter(key_part.astype(jnp.bfloat16), 'dp', scatter_dimension=0...  31.7 us
    mul x6, local copies, waits for them, and re-layouts, recur_heads(): matrix * heads_of(decay)[:, :, None, :]  23.6 us
    reduce_scatter x2, waiting for transfers between devices, body(): lax.psum_scatter(value_part.astype(jnp.bfloat16), 'dp', scatter_dimension...  22.1 us
    dot_general x10, matrix products, truncated_product(): jnp.dot(rescaled_rows, weight, preferred_element_type=jnp.float32)  17.9 us
    mul x4, local copies, waits for them, and re-layouts, recur_heads(): heads_of(value_proj)[..., None] * keys[:, :, None, :]  16 us
    mul x2, local copies, waits for them, and re-layouts, recur_heads(): state_key[..., None] * key_rate[:, :, None, :]  16 us
  transfers between devices with their start and end apart: 12, of which 8 were waited for; matrix products, arithmetic and copies ran while one was open for 40% of the time, Pallas kernels for 0%

commit v1 on v0

v1 whole, which is shorter than its diff:
```python
import functools

import jax
import jax.numpy as jnp
from jax import lax
from jax.experimental import pallas as pl
from jax.experimental.pallas import tpu as pltpu
from jax.sharding import PartitionSpec as P

HEAD = 64
LANES = 128
SPAN = 64
NORM_EPS = 0.25
GROUP_EPS = 0.25
F32 = jnp.float32
BF16 = jnp.bfloat16


def project_kernel(x_ref, gain_ref, q_ref, k_ref, v_ref, g_ref, a_ref, out_ref, acc_ref, sq_ref):
    step = pl.program_id(0)
    last = pl.num_programs(0) - 1
    wide = x_ref[...].astype(F32)
    rows = (wide * gain_ref[0]).astype(BF16)

    @pl.when(step == 0)
    def _():
        acc_ref[...] = jnp.zeros_like(acc_ref)
        sq_ref[...] = jnp.zeros_like(sq_ref)

    sq_ref[...] += jnp.broadcast_to(jnp.sum(wide * wide, axis=1, keepdims=True), sq_ref.shape)
    at = 0
    for w_ref in (q_ref, k_ref, v_ref, g_ref, a_ref):
        cols = w_ref.shape[2]
        acc_ref[:, at : at + cols] += jnp.dot(rows, w_ref[0], preferred_element_type=F32)
        at += cols

    @pl.when(step == last)
    def _():
        out_ref[:, :at] = acc_ref[...].astype(BF16)
        squares = sq_ref[...]
        high = squares.astype(BF16)
        rest = squares - high.astype(F32)
        mid = rest.astype(BF16)
        low = (rest - mid.astype(F32)).astype(BF16)
        lane = lax.broadcasted_iota(jnp.int32, squares.shape, 1)
        packed = jnp.where(lane == 0, high.astype(F32), 0.0)
        packed = jnp.where(lane == 1, mid.astype(F32), packed)
        packed = jnp.where(lane == 2, low.astype(F32), packed)
        out_ref[:, at:] = packed.astype(BF16)


def project(layer, stream, gain, weights):
    batch, depth = stream.shape
    steps = 4
    part = depth // steps
    total = sum(w.shape[2] for w in weights)
    return pl.pallas_call(
        project_kernel,
        grid=(steps,),
        in_specs=[
            pl.BlockSpec((batch, part), lambda i: (0, i)),
            pl.BlockSpec((1, 1, part), lambda i: (layer, 0, i)),
        ]
        + [pl.BlockSpec((1, part, w.shape[2]), lambda i: (layer, i, 0)) for w in weights],
        out_specs=pl.BlockSpec((batch, total + LANES), lambda i: (0, 0)),
        out_shape=jax.ShapeDtypeStruct((batch, total + LANES), BF16),
        scratch_shapes=[pltpu.VMEM((batch, total), F32), pltpu.VMEM((batch, LANES), F32)],
        name=f"project_{layer}",
    )(stream, gain, *weights)


def recur_kernel(
    depth,
    width,
    block_seqs,
    recv_ref,
    pos_ref,
    decay_up_ref,
    rate_up_ref,
    offset_ref,
    hgain_ref,
    state_ref,
    *rest,
):
    mixed_ref, new_ref, q_s, k_s, ku_s, kr_s, d_s, v_s, gate_s, read_s = rest[-10:]
    heads = width // HEAD
    seqs = recv_ref.shape[1]
    step = pl.program_id(0)
    lane = lax.broadcasted_iota(jnp.int32, (1, LANES), 1)
    first = lane < HEAD

    @pl.when(step == 0)
    def _():
        total = recv_ref[0].astype(F32)
        for i in range(1, recv_ref.shape[0]):
            total = total + recv_ref[i].astype(F32)
        at = 4 * width + LANES
        squares = jnp.sum(total[:, at : at + LANES], axis=1, keepdims=True)
        inv = lax.rsqrt(squares / depth + NORM_EPS)
        hidden = total[:, 4 * width : at] * inv
        rank = LANES // 2
        tan = jnp.tanh(hidden[:, :rank])
        logits = offset_ref[0] + jnp.dot(
            tan, decay_up_ref[0], precision=lax.Precision.HIGHEST, preferred_element_type=F32
        )
        soft = jnp.maximum(-logits, 0.0) + jnp.log1p(jnp.exp(-jnp.abs(logits)))
        decay = jnp.exp(-jnp.exp(-soft - 0.5) * pos_ref[...])
        rate = jnp.dot(
            hidden[:, rank:], rate_up_ref[0], precision=lax.Precision.HIGHEST, preferred_element_type=F32
        )
        learn = 1.0 / (1.0 + jnp.exp(-rate))
        gate = total[:, 3 * width : 4 * width] * inv
        gate_s[...] = hgain_ref[0] / (1.0 + jnp.exp(-gate))
        for pair in range(width // LANES):
            for ref, values, base in (
                (q_s, total, 0),
                (k_s, total, width),
                (v_s, total, 2 * width),
                (d_s, decay, None),
                (kr_s, learn, None),
            ):
                lo = (base or 0) + pair * LANES
                x = values[:, lo : lo + LANES]
                if base is not None:
                    x = x * inv
                swapped = pltpu.roll(x, HEAD, 1)
                ref[pl.ds(2 * pair, seqs, stride=heads), :] = jnp.where(first, x, swapped)
                ref[pl.ds(2 * pair + 1, seqs, stride=heads), :] = jnp.where(first, swapped, x)
        keys = k_s[...]
        norm = 0.5 * jnp.sum(keys * keys, axis=1, keepdims=True)
        unit = keys * lax.rsqrt(norm + 1.0)
        ku_s[...] = unit
        kr_s[...] = unit * kr_s[...]

    rows = block_seqs * heads
    own = pl.ds(pl.multiple_of(step * rows, 8), rows)

    def twice(x):
        return jnp.concatenate([x, x], axis=1)

    query, keys, unit, key_rate, decay, value = (
        twice(r[own, :]) for r in (q_s, k_s, ku_s, kr_s, d_s, v_s)
    )
    wide = 2 * LANES
    ones = (
        lax.broadcasted_iota(jnp.int32, (wide, wide), 0) // HEAD
        == lax.broadcasted_iota(jnp.int32, (wide, wide), 1) // HEAD
    ).astype(F32).astype(BF16)
    wlane = lax.broadcasted_iota(jnp.int32, (1, wide), 1)
    group = wlane // HEAD
    within = wlane % HEAD
    readout = jnp.zeros((rows, wide), F32)

    def spread(x):
        return jnp.dot(x.astype(BF16), ones, preferred_element_type=F32)

    for t in range(HEAD * HEAD // wide):
        here = within == 4 * t + group
        old = state_ref[0, :, t * wide : (t + 1) * wide]
        state_key = spread(old * unit)
        values = spread(jnp.where(here, value, 0.0))
        new = old * decay - state_key * key_rate + values * keys
        new_ref[0, :, t * wide : (t + 1) * wide] = new
        readout = jnp.where(here, spread(new * query), readout)
    both = readout[:, :LANES] + readout[:, LANES:]
    both = both + pltpu.roll(both, HEAD, 1)
    mean = jnp.sum(both, axis=1, keepdims=True) / LANES
    centred = both - mean
    var = jnp.sum(centred * centred, axis=1, keepdims=True) / LANES
    read_s[...] = centred * lax.rsqrt(var + GROUP_EPS)
    mine = pl.ds(pl.multiple_of(step * block_seqs, 8), block_seqs)
    for pair in range(width // LANES):
        even = read_s[pl.ds(2 * pair, block_seqs, stride=heads), :]
        odd = read_s[pl.ds(2 * pair + 1, block_seqs, stride=heads), :]
        lanes = slice(pair * LANES, (pair + 1) * LANES)
        mixed_ref[:, lanes] = (jnp.where(first, even, odd) * gate_s[mine, lanes]).astype(BF16)


def recur(layer, depth, received, pos, decay_up, rate_up, offset, head_gain, state, earlier):
    parts, seqs, cols = received.shape
    layers, rows, per_head = state.shape
    width = decay_up.shape[2]
    heads = width // HEAD
    block_seqs = 8
    steps = seqs // block_seqs
    block_rows = block_seqs * heads
    rank = decay_up.shape[1]
    in_specs = [
        pl.BlockSpec((parts, seqs, cols), lambda i: (0, 0, 0)),
        pl.BlockSpec((seqs, 1), lambda i: (0, 0)),
        pl.BlockSpec((1, rank, width), lambda i: (layer, 0, 0)),
        pl.BlockSpec((1, rank, width), lambda i: (layer, 0, 0)),
        pl.BlockSpec((1, 1, width), lambda i: (layer, 0, 0)),
        pl.BlockSpec((1, 1, width), lambda i: (layer, 0, 0)),
        pl.BlockSpec((1, block_rows, per_head), lambda i: (layer, i, 0)),
    ]
    args = [received, pos, decay_up, rate_up, offset, head_gain, state]
    aliases = {}
    if earlier is not None:
        aliases = {len(args): 1}
        in_specs.append(pl.BlockSpec(memory_space=pl.ANY))
        args.append(earlier)
    tall = pltpu.VMEM((rows, LANES), F32)
    return pl.pallas_call(
        functools.partial(recur_kernel, depth, width, block_seqs),
        grid=(steps,),
        in_specs=in_specs,
        out_specs=(
            pl.BlockSpec((block_seqs, width), lambda i: (i, 0)),
            pl.BlockSpec((1, block_rows, per_head), lambda i: (layer, i, 0)),
        ),
        out_shape=(
            jax.ShapeDtypeStruct((seqs, width), BF16),
            jax.ShapeDtypeStruct(state.shape, F32),
        ),
        scratch_shapes=[tall] * 6
        + [pltpu.VMEM((seqs, width), F32), pltpu.VMEM((block_rows, LANES), F32)],
        input_output_aliases=aliases,
        name=f"recur_{layer}",
    )(*args)


def make_body(n_tp, n_dp):
    def body(
        stream,
        history,
        input_norm_gain,
        query_weight,
        key_weight,
        value_weight,
        gate_weight,
        adapter_down_weight,
        decay_up_weight,
        rate_up_weight,
        decay_offset,
        head_norm_gain,
        output_weight,
        recurrent_state,
    ):
        batch, depth_local = stream.shape
        seqs = history.shape[0]
        layers = input_norm_gain.shape[0]
        shape = recurrent_state.shape
        state = recurrent_state.reshape(layers, shape[1] * shape[2], shape[3])
        pos = (0.5 + (history // SPAN % 3).astype(F32))[:, None]
        weights = (query_weight, key_weight, value_weight, gate_weight, adapter_down_weight)
        own_rows = batch // n_tp
        own = lax.dynamic_slice_in_dim(stream, lax.axis_index("tp") * own_rows, own_rows, 0)
        new_state = None
        for layer in range(layers):
            packed = project(layer, stream, input_norm_gain[:, None, :], weights)
            received = lax.all_to_all(packed, "dp", 0, 0, tiled=True)
            mixed, new_state = recur(
                layer,
                depth_local * n_dp,
                received.reshape(n_dp, seqs, -1),
                pos,
                decay_up_weight,
                rate_up_weight,
                decay_offset[:, None, :],
                head_norm_gain[:, None, :],
                state,
                new_state,
            )
            terms = jnp.dot(
                lax.all_gather(mixed, "dp", axis=0, tiled=True),
                output_weight[layer],
                preferred_element_type=F32,
            ).astype(BF16)
            swapped = lax.all_to_all(terms, "tp", 0, 0, tiled=True)
            total = jnp.sum(swapped.reshape(n_tp, own_rows, depth_local).astype(F32), axis=0)
            own = (own.astype(F32) + total).astype(BF16)
            stream = lax.all_gather(own, "tp", axis=0, tiled=True)
        return stream, new_state.reshape(shape)

    return body


def solution(mesh):
    placed = (
        P(None, "dp"),
        P("dp"),
        P(None, "dp"),
        P(None, "dp", "tp"),
        P(None, "dp", "tp"),
        P(None, "dp", "tp"),
        P(None, "dp", "tp"),
        P(None, "dp", None),
        P(None, None, "tp"),
        P(None, None, "tp"),
        P(None, "tp"),
        P(None, "tp"),
        P(None, "tp", "dp"),
        P(None, "dp", "tp", None),
    )
    return jax.shard_map(
        make_body(mesh.shape["tp"], mesh.shape["dp"]),
        mesh=mesh,
        in_specs=placed,
        out_specs=(P(None, "dp"), P(None, "dp", "tp", None)),
        check_vma=False,
    )
```

time: 400 us -> 175 us (0.44)
  waiting for transfers between devices: 189 us -> 17 us
  blocking collectives: 24.9 us -> 101 us
  local copies, waits for them, and re-layouts: 80.6 us -> 4.71 us
  other arithmetic: 44.1 us -> 0.89 us
  matrix products: 44.2 us -> 1.33 us
  Pallas kernels: 0 us -> 37.8 us
  between operations: 14.5 us -> 0.67 us
  starting transfers between devices: 0.68 us -> 10.7 us
    reduce_scatter x10 -> x0, waiting for transfers between devices: 98.2 us -> none  [the longest x2 35.4 us: body(): lax.psum_scatter(query_part.astype(jnp.bfloat16), 'dp', scatter_dimension...]
    psum x2 -> x0, waiting for transfers between devices: 90.5 us -> none  [body(): out_total = lax.psum(terms.astype(jnp.bfloat16), 'tp').astype(jnp.float32)]
    all_gather x0 -> x2, blocking collectives: none -> 63.5 us  [body(): stream = lax.all_gather(own, 'tp', axis=0, tiled=True)]
    mul x12 -> x0, local copies, waits for them, and re-layouts: 55.6 us -> none  [the longest x6 23.6 us: recur_heads(): matrix * heads_of(decay)[:, :, None, :]]
    dot_general x20 -> x2, matrix products: 44.2 us -> 1.33 us  [body(): jnp.dot(lax.all_gather(mixed, 'dp', axis=0, tiled=True), output_weight[la...]
    pallas_call x0 -> x4, Pallas kernels: none -> 37.8 us  [the longest x2 28.7 us: recur(): pl.pallas_call(functools.partial(recur_kernel, depth, width, block_seqs),...]
    all_to_all x0 -> x2, blocking collectives: none -> 26.5 us  [the longest x1 13.7 us: body(): received = lax.all_to_all(packed, 'dp', 0, 0, tiled=True)]
    mul x12 -> x0, other arithmetic: 22.2 us -> none  [the longest x2 9.28 us: recur_heads(): heads_of(value_proj)[..., None] * keys[:, :, None, :]]
  transfers between devices with their start and end apart: 12 -> 2, of which waited for: 8 -> 2; matrix products, arithmetic and copies ran while one was open for 40% -> 1% of each run, Pallas kernels for 0% -> 0%
where the time goes in v1:
time: 175 us; the launch traced here: 174 us
  blocking collectives  101 us (58%)
  Pallas kernels  37.8 us (22%)
  waiting for transfers between devices  17 us (10%)
  starting transfers between devices  10.7 us (6%)
  local copies, waits for them, and re-layouts  4.71 us (3%)
    all_gather x2, blocking collectives, body(): stream = lax.all_gather(own, 'tp', axis=0, tiled=True)  63.5 us
    pallas_call x2, Pallas kernels, recur(): pl.pallas_call(functools.partial(recur_kernel, depth, width, block_seqs),...  28.7 us
    all_to_all x1, blocking collectives, body(): received = lax.all_to_all(packed, 'dp', 0, 0, tiled=True)  13.7 us
    all_to_all x1, blocking collectives, body(): swapped = lax.all_to_all(terms, 'tp', 0, 0, tiled=True)  12.8 us
    all_gather x2, blocking collectives, body(): lax.all_gather(mixed, 'dp', axis=0, tiled=True)  11.2 us
    all_to_all x1, waiting for transfers between devices, body(): swapped = lax.all_to_all(terms, 'tp', 0, 0, tiled=True)  9.43 us
    pallas_call x2, Pallas kernels, project(): pl.pallas_call(project_kernel, grid=(steps,), in_specs=[pl.BlockSpec((bat...  9.11 us
    all_to_all x1, waiting for transfers between devices, body(): received = lax.all_to_all(packed, 'dp', 0, 0, tiled=True)  7.61 us
  transfers between devices with their start and end apart: 2, of which 2 were waited for; matrix products, arithmetic and copies ran while one was open for 1% of the time, Pallas kernels for 0%

profile of v1, /device:TPU:0, one launch (start us, length us, event | category | flops | bytes accessed | tf_op | source)
XLA Modules:
  0.0 174.4 jit_solution(4862259655105508206)
XLA Ops:
  0.6 1.3 broadcast_in_dim.15.gain_ref
  1.9 0.0 copy-start.1
  1.9 0.0 copy-start.2
  1.9 0.0 copy-start.4
  1.9 4.6 %project_0.1 = bf16[128,2304]{1,0:T(8,128)(2,1)} custom-call(bf16[128,1024]{1,0:T(8,128)(2,1)} %x_ref.1, f32[2,1,1024]{2,1,0:T(1,128)} %broadcast_in_dim.15.gain_ref, bf16[2,1024,512]{2,1,0:T(8,128)(2,1)} %q_ref.3, bf16[2,1024,512]{2,1,0:T(8,128)(2,1)} %k_ref.3, bf16[2,1024,512]{2,1,0:T(8,128)(2,1)} %v_ref.3, bf16[2,1024,512]{2,1,0:T(8,128)(2,1)} %g_ref.3, ...), custom_call_target="tpu_custom_call" | custom-call | tf_op jit(solution)/shard_map/project_0/pallas_call | solution.py:57
  6.5 4.3 %all-to-all-start = ((bf16[4,32,2304]{2,1,0:T(8,128)(2,1)}), bf16[4,32,2304]{2,1,0:T(8,128)(2,1)S(1)}, u32[]{:S(2)}, u32[]{:S(2)}) async-start(bf16[4,32,2304]{2,1,0:T(8,128)(2,1)} %bitcast.19), calls=%async_computation | async-start | bytes 1179648 | tf_op jit(solution)/shard_map/all_to_all | solution.py:252
  10.8 0.0 copy-done.1
  10.8 0.6 broadcast_in_dim.17.offset_ref
  11.4 0.0 copy-done.2
  11.4 0.6 broadcast_in_dim.18.hgain_ref
  12.0 0.0 copy-done.4
  12.0 0.7 copy.17.pos_ref
  12.7 7.6 %all-to-all-done.recv_ref = bf16[4,32,2304]{2,1,0:T(8,128)(2,1)S(1)} async-done(((bf16[4,32,2304]{2,1,0:T(8,128)(2,1)}), bf16[4,32,2304]{2,1,0:T(8,128)(2,1)S(1)}, u32[]{:S(2)}, u32[]{:S(2)}) %all-to-all-start) | async-done | bytes 589856 | tf_op jit(solution)/shard_map/all_to_all | solution.py:252
  20.3 0.0 copy-start
  20.3 0.8 copy-done
  21.1 0.0 copy-start.3
  21.1 14.4 %recur_0.1 = (bf16[32,512]{1,0:T(8,128)(2,1)}, f32[2,256,4096]{2,1,0:T(8,128)}) custom-call(bf16[4,32,2304]{2,1,0:T(8,128)(2,1)} %copy-done, f32[32,1]{1,0:T(8,128)} %copy.17.pos_ref, f32[2,64,512]{2,1,0:T(8,128)} %decay_up_ref.3, f32[2,64,512]{2,1,0:T(8,128)} %rate_up_ref.3, f32[2,1,512]{2,1,0:T(1,128)} %broadcast_in_dim.17.offset_ref, ...), custom_call_target="tpu_custom_call" | custom-call | tf_op jit(solution)/shard_map/recur_0/pallas_call | solution.py:204
  35.5 5.6 %all_gather.12 = bf16[128,512]{1,0:T(8,128)(2,1)S(1)} all-gather(bf16[32,512]{1,0:T(8,128)(2,1)} %get-tuple-element.6), channel_id=1, replica_groups=mesh['tp'=8,'dp'=4] {'dp'}, dimensions={0}, use_global_device_ids=true | all-gather | bytes 163840 | tf_op jit(solution)/shard_map/all_gather | solution.py:266
  41.1 0.0 copy-done.3
  41.2 1.0 convolution_convert_fusion.1
  42.2 6.5 %all-to-all-start.1 = ((bf16[8,16,1024]{2,1,0:T(8,128)(2,1)}), bf16[8,16,1024]{2,1,0:T(8,128)(2,1)S(1)}, u32[]{:S(2)}, u32[]{:S(2)}) async-start(bf16[8,16,1024]{2,1,0:T(8,128)(2,1)} %bitcast.4), calls=%async_computation.1 | async-start | bytes 524288 | tf_op jit(solution)/shard_map/all_to_all | solution.py:270
  48.6 9.4 %all-to-all-done.1 = bf16[8,16,1024]{2,1,0:T(8,128)(2,1)S(1)} async-done(((bf16[8,16,1024]{2,1,0:T(8,128)(2,1)}), bf16[8,16,1024]{2,1,0:T(8,128)(2,1)S(1)}, u32[]{:S(2)}, u32[]{:S(2)}) %all-to-all-start.1) | async-done | bytes 262176 | tf_op jit(solution)/shard_map/all_to_all | solution.py:270
  58.1 0.8 add_convert_fusion.1
  58.9 32.7 %all_gather.13.x_ref = bf16[128,1024]{1,0:T(8,128)(2,1)} all-gather(bf16[16,1024]{1,0:T(8,128)(2,1)S(1)} %add_convert_fusion.1), channel_id=1, replica_groups=mesh['tp'=8,'dp'=4] {'tp'}, dimensions={0}, use_global_device_ids=true | all-gather | bytes 294912 | tf_op jit(solution)/shard_map/all_gather | solution.py:273
  91.6 4.5 %project_1.1 = bf16[128,2304]{1,0:T(8,128)(2,1)} custom-call(bf16[128,1024]{1,0:T(8,128)(2,1)} %all_gather.13.x_ref, f32[2,1,1024]{2,1,0:T(1,128)} %broadcast_in_dim.15.gain_ref, bf16[2,1024,512]{2,1,0:T(8,128)(2,1)} %q_ref.3, bf16[2,1024,512]{2,1,0:T(8,128)(2,1)} %k_ref.3, bf16[2,1024,512]{2,1,0:T(8,128)(2,1)} %v_ref.3, bf16[2,1024,512]{2,1,0:T(8,128)(2,1)} %g_ref.3, ...), custom_call_target="tpu_custom_call" | custom-call | tf_op jit(solution)/shard_map/project_1/pallas_call | solution.py:57
  96.2 13.7 %all_to_all.36.recv_ref = bf16[4,32,2304]{2,1,0:T(8,128)(2,1)} all-to-all(bf16[4,32,2304]{2,1,0:T(8,128)(2,1)} %bitcast.20), channel_id=1, replica_groups=mesh['tp'=8,'dp'=4] {'dp'}, dimensions={0} | all-to-all | bytes 1179648 | tf_op jit(solution)/shard_map/all_to_all | solution.py:252
  109.9 14.3 %recur_1.1 = (bf16[32,512]{1,0:T(8,128)(2,1)}, f32[2,256,4096]{2,1,0:T(8,128)}) custom-call(bf16[4,32,2304]{2,1,0:T(8,128)(2,1)} %all_to_all.36.recv_ref, f32[32,1]{1,0:T(8,128)} %copy.17.pos_ref, f32[2,64,512]{2,1,0:T(8,128)} %decay_up_ref.3, f32[2,64,512]{2,1,0:T(8,128)} %rate_up_ref.3, ...), custom_call_target="tpu_custom_call", output_to_operand_aliasing={{1}: (7, {})} | custom-call | tf_op jit(solution)/shard_map/recur_1/pallas_call | solution.py:204
  124.2 5.6 %all_gather.14 = bf16[128,512]{1,0:T(8,128)(2,1)S(1)} all-gather(bf16[32,512]{1,0:T(8,128)(2,1)} %get-tuple-element.8), channel_id=1, replica_groups=mesh['tp'=8,'dp'=4] {'dp'}, dimensions={0}, use_global_device_ids=true | all-gather | bytes 163840 | tf_op jit(solution)/shard_map/all_gather | solution.py:266
  129.8 0.3 convolution_convert_fusion
  130.1 12.8 %all_to_all.37 = bf16[8,16,1024]{2,1,0:T(8,128)(2,1)S(1)} all-to-all(bf16[8,16,1024]{2,1,0:T(8,128)(2,1)S(1)} %bitcast.21), channel_id=1, replica_groups=mesh['tp'=8,'dp'=4] {'tp'}, dimensions={0} | all-to-all | bytes 524288 | tf_op jit(solution)/shard_map/all_to_all | solution.py:270
  143.0 30.7 %all_gather.15 = bf16[128,1024]{1,0:T(8,128)(2,1)S(1)} all-gather(bf16[16,1024]{1,0:T(8,128)(2,1)S(1)} %add_convert_fusion), channel_id=1, replica_groups=mesh['tp'=8,'dp'=4] {'tp'}, dimensions={0}, use_global_device_ids=true | all-gather | bytes 294912 | tf_op jit(solution)/shard_map/all_gather | solution.py:273
  173.7 0.7 copy.21
  (4 shorter events, 0.1 us)
Async XLA Ops:
  1.9 8.9 %copy-start.1 = (f32[2,512]{1,0:T(2,128)S(1)}, f32[2,512]{1,0:T(2,128)}, u32[]{:S(2)}) copy-start(f32[2,512]{1,0:T(2,128)} %param.24) | copy-start | bytes 12292
  1.9 9.5 %copy-start.2 = (f32[2,512]{1,0:T(2,128)S(1)}, f32[2,512]{1,0:T(2,128)}, u32[]{:S(2)}) copy-start(f32[2,512]{1,0:T(2,128)} %param.25) | copy-start | bytes 12292
  1.9 10.0 %copy-start.4 = (s32[32]{0:T(128)S(1)}, s32[32]{0:T(128)}, u32[]{:S(2)}) copy-start(s32[32]{0:T(128)} %param.15) | copy-start | bytes 388
  6.5 13.8 %all-to-all-start = ((bf16[4,32,2304]{2,1,0:T(8,128)(2,1)}), bf16[4,32,2304]{2,1,0:T(8,128)(2,1)S(1)}, u32[]{:S(2)}, u32[]{:S(2)}) async-start(bf16[4,32,2304]{2,1,0:T(8,128)(2,1)} %bitcast.19), calls=%async_computation | async-start | bytes 1179648 | tf_op jit(solution)/shard_map/all_to_all | solution.py:252
  20.3 0.8 copy-start
  21.1 20.0 %copy-start.3 = (bf16[2,512,1024]{2,1,0:T(8,128)(2,1)S(1)}, bf16[2,512,1024]{2,1,0:T(8,128)(2,1)}, u32[]{:S(2)}) copy-start(bf16[2,512,1024]{2,1,0:T(8,128)(2,1)} %param.26) | copy-start | bytes 6291460
  42.2 15.9 %all-to-all-start.1 = ((bf16[8,16,1024]{2,1,0:T(8,128)(2,1)}), bf16[8,16,1024]{2,1,0:T(8,128)(2,1)S(1)}, u32[]{:S(2)}, u32[]{:S(2)}) async-start(bf16[8,16,1024]{2,1,0:T(8,128)(2,1)} %bitcast.4), calls=%async_computation.1 | async-start | bytes 524288 | tf_op jit(solution)/shard_map/all_to_all | solution.py:270
